TPU v7x, 32 devices: a whole 2x2x4 slice. The times are simulated.
32 devices in a mesh: ep: 8 (over z, x), tp: 4 (over y, core).
Axes of the slice: x: 2, y: 2, z: 4, core: 2. Of those that a mesh axis runs over, the one named last changes fastest.
Arguments:
- tokens: bfloat16 [256, 4096], P('ep'), may hold values from -6 to 6
- routes: int32 [256, 4], P('ep'), may hold values from 0 to 7, all different within a row; in each aligned block of 32 rows (0 to 31, 32 to 63, ...) at most 24 rows name the same one
- mix_weights: float32 [256, 4], P('ep'), may hold values from 0.2 to 1
- pre_gain: float32 [4096], replicated, may hold values from 0.1 to 1.9
- gate_weight: bfloat16 [8, 4096, 2048], P('ep', None, 'tp'), may hold values from -0.09375 to 0.09375
- up_weight: bfloat16 [8, 4096, 2048], P('ep', None, 'tp'), may hold values from -0.09375 to 0.09375
- down_weight: bfloat16 [8, 2048, 4096], P('ep', 'tp'), may hold values from -1 to 1
- post_gain: float32 [4096], P('tp'), may hold values from 0.1 to 1.9
Outputs:
- layer_out: bfloat16 [256, 4096], P('ep', 'tp')
Inputs may be any that keep to these rules, and one draw needn't show every extreme that they name: `routes`: within a row the 4 experts differ; among the rows of one index of ep no expert is named more than 24 times.
All inputs are finite; a program needn't handle non-finite values.
Results may differ from a plain program's by a relative error of at most 0.019.
Values may be sent and summed in bfloat16 or wider, within the bound.
No kernel may reach another device: no remote copies, remote signals or barrier semaphores. Data moves between devices by JAX's collectives and lax.ppermute only.
A program may use at most 64 MiB of HBM per device.

v0:
```python
import jax
import jax.numpy as jnp
from jax import lax
from jax.sharding import PartitionSpec as P

epsilon = 1e-06


def on_device(
    tokens, routes, mix_weights, pre_gain, gate_weight, up_weight, down_weight, post_gain
):
    tok_rows, width = tokens.shape
    top_count = routes.shape[1]
    experts = lax.axis_size("ep")
    capacity = min(tok_rows, max(2, (3 * tok_rows * top_count + 2 * experts - 1) // (2 * experts)))
    floats = tokens.astype(jnp.float32)
    normed = (
        floats * lax.rsqrt(jnp.mean(floats * floats, axis=-1, keepdims=True) + epsilon) * pre_gain
    ).astype(jnp.bfloat16)
    chosen = routes.reshape(-1)
    onehot = (chosen[:, None] == jnp.arange(experts, dtype=jnp.int32)[None, :]).astype(jnp.int32)
    before = jnp.cumsum(onehot, axis=0) - onehot
    slot_rank = jnp.sum(before * onehot, axis=1)
    target = chosen * capacity + slot_rank
    placed = target[:, None] == jnp.arange(experts * capacity, dtype=jnp.int32)[None, :]
    by_choice = placed.reshape(tok_rows, top_count, experts * capacity)
    picked = jnp.any(by_choice, axis=1).astype(jnp.bfloat16)
    outgoing = jnp.einsum("tc,td->cd", picked, normed, preferred_element_type=jnp.float32).astype(
        jnp.bfloat16
    )
    outgoing = outgoing.reshape(experts, capacity, width)
    slice_width = width // lax.axis_size("tp")
    outgoing_part = lax.dynamic_slice_in_dim(
        outgoing, lax.axis_index("tp") * slice_width, slice_width, 2
    )
    arrived = lax.all_to_all(outgoing_part, "ep", split_axis=0, concat_axis=0, tiled=True)
    arrived = lax.all_gather(arrived, "tp", axis=2, tiled=True)
    arrived_rows = arrived.reshape(experts * capacity, width)
    gate_act = jnp.dot(arrived_rows, gate_weight[0], preferred_element_type=jnp.float32)
    up_act = jnp.dot(arrived_rows, up_weight[0], preferred_element_type=jnp.float32)
    hidden = (jax.nn.silu(gate_act) * up_act).astype(jnp.bfloat16)
    partial_value = jnp.dot(hidden, down_weight[0], preferred_element_type=jnp.float32)
    summed = lax.psum_scatter(
        partial_value.astype(jnp.bfloat16), "tp", scatter_dimension=1, tiled=True
    )
    returned = lax.all_to_all(
        summed.reshape(experts, capacity, summed.shape[1]),
        "ep",
        split_axis=0,
        concat_axis=0,
        tiled=True,
    )
    results = returned.reshape(experts * capacity, summed.shape[1]).astype(jnp.float32)
    mixing = jnp.sum(mix_weights[:, :, None] * by_choice.astype(jnp.float32), axis=1)
    mixed = jnp.dot(mixing, results, precision=lax.Precision.HIGHEST)
    squares = jnp.sum(mixed * mixed, axis=1)
    total = lax.psum(squares, "tp")
    scale = lax.rsqrt(total / width + epsilon)
    return (mixed * scale[:, None] * post_gain).astype(jnp.bfloat16)


def solution(mesh):
    in_specs = (
        P("ep", None),
        P("ep", None),
        P("ep", None),
        P(),
        P("ep", None, "tp"),
        P("ep", None, "tp"),
        P("ep", "tp", None),
        P("tp"),
    )
    out_specs = P("ep", "tp")
    return jax.shard_map(
        on_device, mesh=mesh, in_specs=in_specs, out_specs=out_specs, check_vma=False
    )
```

profile of v0, /device:TPU:0, one launch (start us, length us, event | category | flops | bytes accessed | tf_op | source)
XLA Modules:
  0.0 118.9 jit_solution(7595916630309548866)
XLA Ops:
  6.5 0.8 copy.21
  7.3 0.1 eq.29
  7.4 0.1 fusion.26
  7.5 0.2 reduce_window_sum.11
  7.7 0.2 select_reduce_fusion.1
  7.8 0.1 reduce_sum.39
  8.0 0.1 copy.22
  8.0 0.7 multiply_add_fusion
  8.7 0.1 fusion.25
  8.8 1.1 fusion.13
  10.0 1.6 %convolution_convert_fusion.1 = bf16[192,4096]{1,0:T(8,128)(2,1)S(1)} fusion(pred[32,192]{1,0:T(8,128)(4,1)S(1)} %fusion.25, bf16[32,4096]{1,0:T(8,128)(2,1)} %param.8, f32[4096]{0:T(1024)} %param.11, f32[32]{0:T(128)S(1)} %add_rsqrt_fusion.1), kind=kOutput, calls=%fused_computation.1 | convolution fusion | flops 51642368 | bytes 1857664 | tf_op jit(solution)/shard_map/tc,td->cd/dot_general | solution.py:28
  11.6 19.2 %all_to_all.10 = bf16[8,24,1024]{2,1,0:T(8,128)(2,1)} all-to-all(bf16[8,24,1024]{2,1,0:T(8,128)(2,1)S(1)} %constant_dynamic-slice_fusion), channel_id=1, replica_groups=mesh['ep'=8,'tp'=4] {'ep'}, dimensions={0} | all-to-all | bytes 786432 | tf_op jit(solution)/shard_map/all_to_all | solution.py:36
  30.8 0.0 all-gather.2.cloned.1.call-update
  30.9 0.0 reduce-scatter.2.cloned.1.call-start
  30.9 18.4 %all-gather.2.cloned.1.call-done = bf16[8,24,4096]{2,1,0:T(8,128)(2,1)} async-done(((bf16[8,24,1024]{2,1,0:T(8,128)(2,1)}), bf16[8,24,4096]{2,1,0:T(8,128)(2,1)}) %all-gather.2.cloned.1.call-update) | async-done | bytes 1572880 | tf_op jit(solution)/shard_map/all_gather | solution.py:37
  49.4 3.7 %fusion.3 = f32[192,512]{1,0:T(8,128)S(1)} fusion(bf16[192,4096]{1,0:T(8,128)(2,1)} %bitcast.26, bf16[1,4096,512]{2,1,0:T(8,128)(2,1)} %param.12), kind=kOutput, calls=%fused_computation.5 | convolution fusion | flops 805306368 | bytes 6160384 | tf_op jit(solution)/shard_map/dot_general | solution.py:39
  53.1 6.6 %convolution_convert_fusion = bf16[192,4096]{1,0:T(8,128)(2,1)} fusion(bf16[1,512,4096]{2,1,0:T(8,128)(2,1)} %param.14, bf16[192,4096]{1,0:T(8,128)(2,1)S(1)} %bitcast.27, bf16[1,4096,512]{2,1,0:T(8,128)(2,1)} %param.13, f32[192,512]{1,0:T(8,128)S(1)} %fusion.3), kind=kOutput, calls=%fused_computation | convolution fusion | flops 1611988992 | bytes 11927552 | tf_op jit(solution)/shard_map/dot_general | solution.py:42
  59.8 28.1 %reduce-scatter.2.cloned.1.call-done = bf16[192,1024]{1,0:T(8,128)(2,1)} async-done(((bf16[192,4096]{1,0:T(8,128)(2,1)}), bf16[192,1024]{1,0:T(8,128)(2,1)}) %reduce-scatter.2.cloned.1.call-update) | async-done | bytes 393232 | tf_op jit(solution)/shard_map/reduce_scatter | solution.py:43
  87.9 5.5 %all-to-all-start.1 = ((bf16[8,24,1024]{2,1,0:T(8,128)(2,1)}), bf16[8,24,1024]{2,1,0:T(8,128)(2,1)S(1)}, u32[]{:S(2)}, u32[]{:S(2)}) async-start(bf16[8,24,1024]{2,1,0:T(8,128)(2,1)} %bitcast.28), calls=%async_computation.2 | async-start | bytes 786432 | tf_op jit(solution)/shard_map/all_to_all | solution.py:46
  93.4 0.1 select_reduce_fusion
  93.5 11.5 %all-to-all-done.1 = bf16[8,24,1024]{2,1,0:T(8,128)(2,1)S(1)} async-done(((bf16[8,24,1024]{2,1,0:T(8,128)(2,1)}), bf16[8,24,1024]{2,1,0:T(8,128)(2,1)S(1)}, u32[]{:S(2)}, u32[]{:S(2)}) %all-to-all-start.1) | async-done | bytes 393248 | tf_op jit(solution)/shard_map/all_to_all | solution.py:46
  105.0 0.4 multiply_reduce_fusion
  105.4 5.9 %psum.7 = f32[32]{0:T(128)S(1)} all-reduce(f32[32]{0:T(128)S(1)} %get-tuple-element.5), channel_id=1, replica_groups=mesh['ep'=8,'tp'=4] {'tp'}, use_global_device_ids=true, to_apply=%region_7.8 | all-reduce | flops 32 | bytes 256 | tf_op jit(solution)/shard_map/psum | solution.py:57
  111.3 0.7 multiply_convert_fusion
  (11 shorter events, 0.1 us)
Async XLA Ops:
  6.5 42.8 %all-gather.2.cloned.1.call-start = ((), (), s32[]{:S(2)}) async-start(), calls=%async_computation.3 | async-start | bytes 1966080 | tf_op jit(solution)/shard_map/all_gather | solution.py:37
  30.9 57.1 %reduce-scatter.2.cloned.1.call-start = ((), (), s32[]{:S(2)}) async-start(), calls=%async_computation.4 | async-start | bytes 1966080 | tf_op jit(solution)/shard_map/reduce_scatter | solution.py:43
  49.4 3.8 %copy-start = (bf16[8,24,4096]{2,1,0:T(8,128)(2,1)S(1)}, bf16[8,24,4096]{2,1,0:T(8,128)(2,1)}, u32[]{:S(2)}) copy-start(bf16[8,24,4096]{2,1,0:T(8,128)(2,1)} %all-gather.2.cloned.1.call-done) | copy-start | bytes 4718596
  53.1 40.3 %copy-start.2 = (f32[32,4]{0,1:T(4,128)S(1)}, f32[32,4]{0,1:T(4,128)}, u32[]{:S(2)}) copy-start(f32[32,4]{0,1:T(4,128)} %param.10) | copy-start | bytes 1540
  53.1 58.2 %copy-start.1 = (f32[1024]{0:T(1024)S(1)}, f32[1024]{0:T(1024)}, u32[]{:S(2)}) copy-start(f32[1024]{0:T(1024)} %param.15) | copy-start | bytes 12292
  87.9 17.1 %all-to-all-start.1 = ((bf16[8,24,1024]{2,1,0:T(8,128)(2,1)}), bf16[8,24,1024]{2,1,0:T(8,128)(2,1)S(1)}, u32[]{:S(2)}, u32[]{:S(2)}) async-start(bf16[8,24,1024]{2,1,0:T(8,128)(2,1)} %bitcast.28), calls=%async_computation.2 | async-start | bytes 786432 | tf_op jit(solution)/shard_map/all_to_all | solution.py:46
Sparse Core Ops, SparseCore 0:
  31.0 18.3 all-gather.1
  59.9 27.9 reduce-scatter.1
where the time goes:
time: 119 us
  waiting for transfers between devices  58.1 us (49%)
  blocking collectives  25.2 us (21%)
  between operations  13.5 us (11%)
  matrix products  12.3 us (10%)
  starting transfers between devices  5.53 us (5%)
  other arithmetic  3.16 us (3%)
    reduce_scatter x1, waiting for transfers between devices, on_device(): lax.psum_scatter(partial_value.astype(jnp.bfloat16), 'tp', scatter_dimens...  28.1 us
    all_to_all x1, blocking collectives, on_device(): lax.all_to_all(outgoing_part, 'ep', split_axis=0, concat_axis=0, tiled=True)  19.2 us
    all_gather x1, waiting for transfers between devices, on_device(): arrived = lax.all_gather(arrived, 'tp', axis=2, tiled=True)  18.4 us
    all_to_all x1, waiting for transfers between devices, on_device(): lax.all_to_all(summed.reshape(experts, capacity, summed.shape[1]), 'ep',...  11.5 us
    dot_general x1, matrix products, on_device(): jnp.dot(hidden, down_weight[0], preferred_element_type=jnp.float32)  6.61 us
    psum x1, blocking collectives, on_device(): total = lax.psum(squares, 'tp')  5.95 us
    all_to_all x1, starting transfers between devices, on_device(): lax.all_to_all(summed.reshape(experts, capacity, summed.shape[1]), 'ep',...  5.48 us
    dot_general x1, matrix products, on_device(): jnp.dot(arrived_rows, gate_weight[0], preferred_element_type=jnp.float32)  3.75 us
  transfers between devices with their start and end apart: 3, of which 3 were waited for; matrix products, arithmetic and copies ran while one was open for 0% of the time, Pallas kernels for 0%

commit v1 on v0

v1 whole, which is shorter than its diff:
```python
import jax
import jax.numpy as jnp
from jax import lax
from jax.sharding import PartitionSpec as P

epsilon = 1e-06
direct_limit = 16


def send(value, axis, move):
    size = lax.axis_size(axis)
    return lax.ppermute(value, axis, [(i, move(i, size)) for i in range(size)])


def on_device(
    tokens, routes, mix_weights, pre_gain, gate_weight, up_weight, down_weight, post_gain
):
    tok_rows, width = tokens.shape
    top_count = routes.shape[1]
    experts = lax.axis_size("ep")
    shards = lax.axis_size("tp")
    chips = shards // 2
    piece = width // shards
    half = width // 2
    direct = experts <= direct_limit
    capacity = min(tok_rows, max(2, (3 * tok_rows * top_count + 2 * experts - 1) // (2 * experts)))
    slots = experts * capacity
    core = lax.axis_index("tp") % 2
    chip = lax.axis_index("tp") // 2

    def exchange(rows, back):
        if not direct:
            blocks = rows.reshape(experts, capacity, rows.shape[1])
            blocks = lax.all_to_all(blocks, "ep", split_axis=0, concat_axis=0, tiled=True)
            return blocks.reshape(rows.shape)
        sign = -1 if back else 1
        parts = [rows[:capacity]]
        for k in range(1, experts):
            block = rows[k * capacity : (k + 1) * capacity]
            parts.append(send(block, "ep", lambda i, n, k=k: (i + sign * k) % n))
        return jnp.concatenate(parts, axis=0)

    chosen = routes.reshape(-1)
    if direct:
        chosen = (chosen - lax.axis_index("ep")) % experts
    onehot = (chosen[:, None] == jnp.arange(experts, dtype=jnp.int32)[None, :]).astype(jnp.float32)
    count = tok_rows * top_count
    earlier = (
        jnp.arange(count, dtype=jnp.int32)[:, None] > jnp.arange(count, dtype=jnp.int32)[None, :]
    ).astype(jnp.float32)
    before = jnp.dot(earlier, onehot, preferred_element_type=jnp.float32)
    slot_rank = jnp.sum(before * onehot, axis=1).astype(jnp.int32)
    target = (chosen * capacity + slot_rank).reshape(tok_rows, top_count)
    by_choice = target[:, :, None] == jnp.arange(slots, dtype=jnp.int32)[None, None, :]
    picked = jnp.any(by_choice, axis=1).astype(jnp.bfloat16)
    mixing = jnp.sum(jnp.where(by_choice, mix_weights[:, :, None], 0.0), axis=1)

    floats = tokens.astype(jnp.float32)
    scale = lax.rsqrt(jnp.mean(floats * floats, axis=-1, keepdims=True) + epsilon)
    own_half = lax.dynamic_slice_in_dim(tokens, core * half, half, 1).astype(jnp.float32)
    own_gain = lax.dynamic_slice_in_dim(pre_gain, core * half, half, 0)
    normed = (own_half * scale * own_gain).astype(jnp.bfloat16)
    outgoing = jnp.dot(picked.T, normed, preferred_element_type=jnp.float32).astype(jnp.bfloat16)
    mine = exchange(outgoing, False)
    other = send(mine, "tp", lambda i, n: i ^ 1)
    is_first = core == 0
    arrived = jnp.concatenate(
        [jnp.where(is_first, mine, other), jnp.where(is_first, other, mine)], axis=1
    )
    gate_act = jnp.dot(arrived, gate_weight[0], preferred_element_type=jnp.float32)
    up_act = jnp.dot(arrived, up_weight[0], preferred_element_type=jnp.float32)
    hidden = (jax.nn.silu(gate_act) * up_act).astype(jnp.bfloat16)
    partial_value = jnp.dot(hidden, down_weight[0], preferred_element_type=jnp.float32)
    partial_value = partial_value.astype(jnp.bfloat16)
    firsts = jnp.concatenate(
        [partial_value[:, (2 * j) * piece : (2 * j + 1) * piece] for j in range(chips)], axis=1
    )
    seconds = jnp.concatenate(
        [partial_value[:, (2 * j + 1) * piece : (2 * j + 2) * piece] for j in range(chips)], axis=1
    )
    kept = jnp.where(is_first, firsts, seconds)
    given = jnp.where(is_first, seconds, firsts)
    gained = send(given, "tp", lambda i, n: i ^ 1)
    chip_sum = (kept.astype(jnp.float32) + gained.astype(jnp.float32)).astype(jnp.bfloat16)
    returned = exchange(chip_sum, True)
    mixed_part = jnp.dot(mixing, returned.astype(jnp.float32), precision=lax.Precision.HIGHEST)
    mixed_sent = mixed_part.astype(jnp.bfloat16)
    mixed = mixed_part
    for k in range(1, chips):
        mixed = mixed + send(mixed_sent, "tp", lambda i, n, k=k: (i + 2 * k) % n).astype(jnp.float32)
    squares = jnp.sum(mixed * mixed, axis=1, keepdims=True)
    squares = jnp.broadcast_to(squares, (tok_rows, 128))
    total = squares + send(squares, "tp", lambda i, n: i ^ 1)
    scale_out = lax.rsqrt(total[:, :1] / width + epsilon)
    result = lax.dynamic_slice_in_dim(mixed, chip * piece, piece, 1)
    return (result * scale_out * post_gain).astype(jnp.bfloat16)


def solution(mesh):
    in_specs = (
        P("ep", None),
        P("ep", None),
        P("ep", None),
        P(),
        P("ep", None, "tp"),
        P("ep", None, "tp"),
        P("ep", "tp", None),
        P("tp"),
    )
    out_specs = P("ep", "tp")
    return jax.shard_map(
        on_device, mesh=mesh, in_specs=in_specs, out_specs=out_specs, check_vma=False
    )
```

time: 119 us -> 73.2 us (0.62)
  waiting for transfers between devices: 58.1 us -> 25.8 us
  starting transfers between devices: 5.53 us -> 31.2 us
  blocking collectives: 25.2 us -> 0 us
  between operations: 13.5 us -> 0.29 us
  matrix products: 12.3 us -> 10.5 us
    ppermute x0 -> x18, starting transfers between devices: none -> 31.2 us  [send(): return lax.ppermute(value, axis, [(i, move(i, size)) for i in range(size)])]
    reduce_scatter x1 -> x0, waiting for transfers between devices: 28.1 us -> none  [on_device(): lax.psum_scatter(partial_value.astype(jnp.bfloat16), 'tp', scatter_dimens...]
    ppermute x0 -> x18, waiting for transfers between devices: none -> 25.8 us  [send(): return lax.ppermute(value, axis, [(i, move(i, size)) for i in range(size)])]
    all_to_all x1 -> x0, blocking collectives: 19.2 us -> none  [on_device(): lax.all_to_all(outgoing_part, 'ep', split_axis=0, concat_axis=0, tiled=True)]
    all_gather x1 -> x0, waiting for transfers between devices: 18.4 us -> none  [on_device(): arrived = lax.all_gather(arrived, 'tp', axis=2, tiled=True)]
    all_to_all x1 -> x0, waiting for transfers between devices: 11.5 us -> none  [on_device(): lax.all_to_all(summed.reshape(experts, capacity, summed.shape[1]), 'ep',...]
    psum x1 -> x0, blocking collectives: 5.95 us -> none  [on_device(): total = lax.psum(squares, 'tp')]
    all_to_all x1 -> x0, starting transfers between devices: 5.48 us -> none  [on_device(): lax.all_to_all(summed.reshape(experts, capacity, summed.shape[1]), 'ep',...]
  transfers between devices with their start and end apart: 3 -> 18, of which waited for: 3 -> 10; matrix products, arithmetic and copies ran while one was open for 0% -> 0% of each run, Pallas kernels for 0% -> 0%
where the time goes in v1:
time: 73.2 us; the launch traced here: 72.9 us
  starting transfers between devices  31.2 us (43%)
  waiting for transfers between devices  25.8 us (35%)
  matrix products  10.5 us (14%)
  other arithmetic  2.98 us (4%)
  local copies, waits for them, and re-layouts  2.15 us (3%)
    ppermute x18, starting transfers between devices, send(): return lax.ppermute(value, axis, [(i, move(i, size)) for i in range(size)])  31.2 us
    ppermute x18, waiting for transfers between devices, send(): return lax.ppermute(value, axis, [(i, move(i, size)) for i in range(size)])  25.8 us
    dot_general x1, matrix products, on_device(): jnp.dot(hidden, down_weight[0], preferred_element_type=jnp.float32)  5.42 us
    dot_general x1, matrix products, on_device(): up_act = jnp.dot(arrived, up_weight[0], preferred_element_type=jnp.float32)  3.16 us
  transfers between devices with their start and end apart: 18, of which 10 were waited for; matrix products, arithmetic and copies ran while one was open for 0% of the time, Pallas kernels for 0%

profile of v1, /device:TPU:0, one launch (start us, length us, event | category | flops | bytes accessed | tf_op | source)
XLA Modules:
  0.0 72.9 jit_solution(13574756000722302208)
XLA Ops:
  1.4 1.1 %multiply_reduce_fusion = f32[32]{0:T(128)S(1)} fusion(bf16[32,4096]{1,0:T(8,128)(2,1)} %param.8), kind=kLoop, calls=%fused_computation.16 | loop fusion | flops 393184 | bytes 262272 | tf_op jit(solution)/shard_map/reduce_sum | solution.py:59
  3.2 1.3 %convolution_convert_fusion.1 = bf16[192,2048]{1,0:T(8,128)(2,1)S(1)} fusion(pred[32,192]{1,0:T(8,128)(4,1)S(1)} %fusion.14, f32[2048]{0:T(1024)S(1)} %dynamic_slice.10, f32[32]{0:T(128)S(1)} %add_rsqrt_fusion, bf16[32,4096]{1,0:T(8,128)(2,1)} %param.8, s32[]{:T(128)S(6)} %select_n.61), kind=kOutput, calls=%fused_computation.6 | convolution fusion | flops 25821184 | bytes 931972 | tf_op jit(solution)/shard_map/dot_general | solution.py:63
  4.6 3.0 %collective-permute-start = (bf16[24,2048]{1,0:T(8,128)(2,1)S(1)}, bf16[24,2048]{1,0:T(8,128)(2,1)S(1)}, u32[]{:S(2)}, u32[]{:S(2)}) collective-permute-start(bf16[24,2048]{1,0:T(8,128)(2,1)S(1)} %get-tuple-element.27), channel_id=1, source_target_pairs={{0,4},{4,8},{8,12},{12,16},{16,20},{20,24},{24,28},{28,0},{1,5},{5... | collective-permute-start | bytes 294920 | tf_op jit(solution)/shard_map/ppermute | solution.py:12
  7.6 1.6 %collective-permute-start.1 = (bf16[24,2048]{1,0:T(8,128)(2,1)S(1)}, bf16[24,2048]{1,0:T(8,128)(2,1)S(1)}, u32[]{:S(2)}, u32[]{:S(2)}) collective-permute-start(bf16[24,2048]{1,0:T(8,128)(2,1)S(1)} %get-tuple-element.26), channel_id=1, source_target_pairs={{0,8},{4,12},{8,16},{12,20},{16,24},{20,28},{24,0},{28,4},{1,9},{5... | collective-permute-start | bytes 294920 | tf_op jit(solution)/shard_map/ppermute | solution.py:12
  9.2 2.6 %collective-permute-start.2 = (bf16[24,2048]{1,0:T(8,128)(2,1)S(1)}, bf16[24,2048]{1,0:T(8,128)(2,1)S(1)}, u32[]{:S(2)}, u32[]{:S(2)}) collective-permute-start(bf16[24,2048]{1,0:T(8,128)(2,1)S(1)} %get-tuple-element.25), channel_id=1, source_target_pairs={{0,12},{4,16},{8,20},{12,24},{16,28},{20,0},{24,4},{28,8},{1,13},{... | collective-permute-start | bytes 294920 | tf_op jit(solution)/shard_map/ppermute | solution.py:12
  11.8 1.2 %collective-permute-start.3 = (bf16[24,2048]{1,0:T(8,128)(2,1)S(1)}, bf16[24,2048]{1,0:T(8,128)(2,1)S(1)}, u32[]{:S(2)}, u32[]{:S(2)}) collective-permute-start(bf16[24,2048]{1,0:T(8,128)(2,1)S(1)} %get-tuple-element.24), channel_id=1, source_target_pairs={{0,16},{4,20},{8,24},{12,28},{16,0},{20,4},{24,8},{28,12},{1,17},{... | collective-permute-start | bytes 294920 | tf_op jit(solution)/shard_map/ppermute | solution.py:12
  13.0 2.6 %collective-permute-start.4 = (bf16[24,2048]{1,0:T(8,128)(2,1)S(1)}, bf16[24,2048]{1,0:T(8,128)(2,1)S(1)}, u32[]{:S(2)}, u32[]{:S(2)}) collective-permute-start(bf16[24,2048]{1,0:T(8,128)(2,1)S(1)} %get-tuple-element.23), channel_id=1, source_target_pairs={{0,20},{4,24},{8,28},{12,0},{16,4},{20,8},{24,12},{28,16},{1,21},{... | collective-permute-start | bytes 294920 | tf_op jit(solution)/shard_map/ppermute | solution.py:12
  15.6 1.3 %collective-permute-start.5 = (bf16[24,2048]{1,0:T(8,128)(2,1)S(1)}, bf16[24,2048]{1,0:T(8,128)(2,1)S(1)}, u32[]{:S(2)}, u32[]{:S(2)}) collective-permute-start(bf16[24,2048]{1,0:T(8,128)(2,1)S(1)} %get-tuple-element.22), channel_id=1, source_target_pairs={{0,24},{4,28},{8,0},{12,4},{16,8},{20,12},{24,16},{28,20},{1,25},{... | collective-permute-start | bytes 294920 | tf_op jit(solution)/shard_map/ppermute | solution.py:12
  17.0 1.5 %collective-permute-start.6 = (bf16[24,2048]{1,0:T(8,128)(2,1)S(1)}, bf16[24,2048]{1,0:T(8,128)(2,1)S(1)}, u32[]{:S(2)}, u32[]{:S(2)}) collective-permute-start(bf16[24,2048]{1,0:T(8,128)(2,1)S(1)} %get-tuple-element.21), channel_id=1, source_target_pairs={{0,28},{4,0},{8,4},{12,8},{16,12},{20,16},{24,20},{28,24},{1,29},{... | collective-permute-start | bytes 294920 | tf_op jit(solution)/shard_map/ppermute | solution.py:12
  18.5 3.6 %collective-permute-done.2 = bf16[24,2048]{1,0:T(8,128)(2,1)S(1)} collective-permute-done((bf16[24,2048]{1,0:T(8,128)(2,1)S(1)}, bf16[24,2048]{1,0:T(8,128)(2,1)S(1)}, u32[]{:S(2)}, u32[]{:S(2)}) %collective-permute-start.2) | collective-permute-done | bytes 98336 | tf_op jit(solution)/shard_map/ppermute | solution.py:12
  23.0 2.3 %collective-permute-done.7 = bf16[192,2048]{1,0:T(8,128)(2,1)S(1)} collective-permute-done((bf16[192,2048]{1,0:T(8,128)(2,1)S(1)}, bf16[192,2048]{1,0:T(8,128)(2,1)S(1)}, u32[]{:S(2)}, u32[]{:S(2)}) %collective-permute-start.7) | collective-permute-done | bytes 786464 | tf_op jit(solution)/shard_map/ppermute | solution.py:12
  25.4 3.2 %fusion.1 = f32[192,512]{1,0:T(8,128)S(1)} fusion(bf16[1,4096,512]{2,1,0:T(8,128)(2,1)} %param.13, bf16[192,2048]{1,0:T(8,128)(2,1)S(1)} %get-tuple-element.12, bf16[192,2048]{1,0:T(8,128)(2,1)S(1)} %get-tuple-element.11), kind=kOutput, calls=%fused_computation.2 | convolution fusion | flops 808452096 | bytes 6160384 | tf_op jit(solution)/shard_map/dot_general | solution.py:71
  28.6 5.4 %convolution_convert_fusion = bf16[192,4096]{1,0:T(8,128)(2,1)S(1)} fusion(bf16[1,512,4096]{2,1,0:T(8,128)(2,1)} %param.14, f32[192,512]{1,0:T(8,128)S(1)} %fusion.1, bf16[1,4096,512]{2,1,0:T(8,128)(2,1)} %param.12, bf16[192,2048]{1,0:T(8,128)(2,1)S(1)} %get-tuple-element.12, bf16[192,2048]{1,0:T(8,128)(2,1)S(1)} %get-tuple-element.11), kind=kOutput, calls=%fused_computation | convolution fusion | flops 1615134720 | bytes 11927552 | tf_op jit(solution)/shard_map/dot_general | solution.py:73
  34.6 2.1 %collective-permute-done.8 = bf16[192,2048]{1,0:T(8,128)(2,1)S(1)} collective-permute-done((bf16[192,2048]{1,0:T(8,128)(2,1)S(1)}, bf16[192,2048]{1,0:T(8,128)(2,1)S(1)}, u32[]{:S(2)}, u32[]{:S(2)}) %collective-permute-start.8) | collective-permute-done | bytes 786464 | tf_op jit(solution)/shard_map/ppermute | solution.py:12
  37.2 8.2 %collective-permute-start.9 = (bf16[24,2048]{1,0:T(8,128)(2,1)S(1)}, bf16[24,2048]{1,0:T(8,128)(2,1)S(1)}, u32[]{:S(2)}, u32[]{:S(2)}) collective-permute-start(bf16[24,2048]{1,0:T(8,128)(2,1)S(1)} %get-tuple-element.19), channel_id=1, source_target_pairs={{0,28},{4,0},{8,4},{12,8},{16,12},{20,16},{24,20},{28,24},{1,29},{... | collective-permute-start | bytes 294920 | tf_op jit(solution)/shard_map/ppermute | solution.py:12
  45.6 1.6 %collective-permute-start.10 = (bf16[24,2048]{1,0:T(8,128)(2,1)S(1)}, bf16[24,2048]{1,0:T(8,128)(2,1)S(1)}, u32[]{:S(2)}, u32[]{:S(2)}) collective-permute-start(bf16[24,2048]{1,0:T(8,128)(2,1)S(1)} %get-tuple-element.18), channel_id=1, source_target_pairs={{0,24},{4,28},{8,0},{12,4},{16,8},{20,12},{24,16},{28,20},{1,25},{... | collective-permute-start | bytes 294920 | tf_op jit(solution)/shard_map/ppermute | solution.py:12
  47.2 1.9 %collective-permute-start.12 = (bf16[24,2048]{1,0:T(8,128)(2,1)S(1)}, bf16[24,2048]{1,0:T(8,128)(2,1)S(1)}, u32[]{:S(2)}, u32[]{:S(2)}) collective-permute-start(bf16[24,2048]{1,0:T(8,128)(2,1)S(1)} %get-tuple-element.16), channel_id=1, source_target_pairs={{0,16},{4,20},{8,24},{12,28},{16,0},{20,4},{24,8},{28,12},{1,17},{... | collective-permute-start | bytes 294920 | tf_op jit(solution)/shard_map/ppermute | solution.py:12
  49.1 1.0 %collective-permute-start.13 = (bf16[24,2048]{1,0:T(8,128)(2,1)S(1)}, bf16[24,2048]{1,0:T(8,128)(2,1)S(1)}, u32[]{:S(2)}, u32[]{:S(2)}) collective-permute-start(bf16[24,2048]{1,0:T(8,128)(2,1)S(1)} %get-tuple-element.15), channel_id=1, source_target_pairs={{0,12},{4,16},{8,20},{12,24},{16,28},{20,0},{24,4},{28,8},{1,13},{... | collective-permute-start | bytes 294920 | tf_op jit(solution)/shard_map/ppermute | solution.py:12
  50.1 2.0 %collective-permute-start.14 = (bf16[24,2048]{1,0:T(8,128)(2,1)S(1)}, bf16[24,2048]{1,0:T(8,128)(2,1)S(1)}, u32[]{:S(2)}, u32[]{:S(2)}) collective-permute-start(bf16[24,2048]{1,0:T(8,128)(2,1)S(1)} %get-tuple-element.14), channel_id=1, source_target_pairs={{0,8},{4,12},{8,16},{12,20},{16,24},{20,28},{24,0},{28,4},{1,9},{5... | collective-permute-start | bytes 294920 | tf_op jit(solution)/shard_map/ppermute | solution.py:12
  53.3 10.4 %collective-permute-done.12 = bf16[24,2048]{1,0:T(8,128)(2,1)S(1)} collective-permute-done((bf16[24,2048]{1,0:T(8,128)(2,1)S(1)}, bf16[24,2048]{1,0:T(8,128)(2,1)S(1)}, u32[]{:S(2)}, u32[]{:S(2)}) %collective-permute-start.12) | collective-permute-done | bytes 98336 | tf_op jit(solution)/shard_map/ppermute | solution.py:12
  63.7 1.4 %collective-permute-done.13 = bf16[24,2048]{1,0:T(8,128)(2,1)S(1)} collective-permute-done((bf16[24,2048]{1,0:T(8,128)(2,1)S(1)}, bf16[24,2048]{1,0:T(8,128)(2,1)S(1)}, u32[]{:S(2)}, u32[]{:S(2)}) %collective-permute-start.13) | collective-permute-done | bytes 98336 | tf_op jit(solution)/shard_map/ppermute | solution.py:12
  65.7 1.6 %collective-permute-start.16 = (bf16[32,2048]{1,0:T(8,128)(2,1)S(1)}, bf16[32,2048]{1,0:T(8,128)(2,1)S(1)}, u32[]{:S(2)}, u32[]{:S(2)}) collective-permute-start(bf16[32,2048]{1,0:T(8,128)(2,1)S(1)} %get-tuple-element.29), channel_id=1, source_target_pairs={{0,2},{1,3},{2,0},{3,1},{4,6},{5,7},{6,4},{7,5},{8,10},{9,11},{10,... | collective-permute-start | bytes 393224 | tf_op jit(solution)/shard_map/ppermute | solution.py:12
  67.3 3.5 %collective-permute-done.16 = bf16[32,2048]{1,0:T(8,128)(2,1)S(1)} collective-permute-done((bf16[32,2048]{1,0:T(8,128)(2,1)S(1)}, bf16[32,2048]{1,0:T(8,128)(2,1)S(1)}, u32[]{:S(2)}, u32[]{:S(2)}) %collective-permute-start.16) | collective-permute-done | bytes 131104 | tf_op jit(solution)/shard_map/ppermute | solution.py:12
  71.0 1.2 %collective-permute-done.17 = f32[32,128]{0,1:T(8,128)S(1)} collective-permute-done((f32[32,128]{0,1:T(8,128)S(1)}, f32[32,128]{0,1:T(8,128)S(1)}, u32[]{:S(2)}, u32[]{:S(2)}) %collective-permute-start.17) | collective-permute-done | bytes 16416 | tf_op jit(solution)/shard_map/ppermute | solution.py:12
  (58 shorter events, 6.8 us)
Async XLA Ops:
  4.6 11.0 %collective-permute-start = (bf16[24,2048]{1,0:T(8,128)(2,1)S(1)}, bf16[24,2048]{1,0:T(8,128)(2,1)S(1)}, u32[]{:S(2)}, u32[]{:S(2)}) collective-permute-start(bf16[24,2048]{1,0:T(8,128)(2,1)S(1)} %get-tuple-element.27), channel_id=1, source_target_pairs={{0,4},{4,8},{8,12},{12,16},{16,20},{20,24},{24,28},{28,0},{1,5},{5... | collective-permute-start | bytes 294920 | tf_op jit(solution)/shard_map/ppermute | solution.py:12
  7.6 9.4 %collective-permute-start.1 = (bf16[24,2048]{1,0:T(8,128)(2,1)S(1)}, bf16[24,2048]{1,0:T(8,128)(2,1)S(1)}, u32[]{:S(2)}, u32[]{:S(2)}) collective-permute-start(bf16[24,2048]{1,0:T(8,128)(2,1)S(1)} %get-tuple-element.26), channel_id=1, source_target_pairs={{0,8},{4,12},{8,16},{12,20},{16,24},{20,28},{24,0},{28,4},{1,9},{5... | collective-permute-start | bytes 294920 | tf_op jit(solution)/shard_map/ppermute | solution.py:12
  9.2 12.9 %collective-permute-start.2 = (bf16[24,2048]{1,0:T(8,128)(2,1)S(1)}, bf16[24,2048]{1,0:T(8,128)(2,1)S(1)}, u32[]{:S(2)}, u32[]{:S(2)}) collective-permute-start(bf16[24,2048]{1,0:T(8,128)(2,1)S(1)} %get-tuple-element.25), channel_id=1, source_target_pairs={{0,12},{4,16},{8,20},{12,24},{16,28},{20,0},{24,4},{28,8},{1,13},{... | collective-permute-start | bytes 294920 | tf_op jit(solution)/shard_map/ppermute | solution.py:12
  11.8 10.9 %collective-permute-start.3 = (bf16[24,2048]{1,0:T(8,128)(2,1)S(1)}, bf16[24,2048]{1,0:T(8,128)(2,1)S(1)}, u32[]{:S(2)}, u32[]{:S(2)}) collective-permute-start(bf16[24,2048]{1,0:T(8,128)(2,1)S(1)} %get-tuple-element.24), channel_id=1, source_target_pairs={{0,16},{4,20},{8,24},{12,28},{16,0},{20,4},{24,8},{28,12},{1,17},{... | collective-permute-start | bytes 294920 | tf_op jit(solution)/shard_map/ppermute | solution.py:12
  13.0 9.7 %collective-permute-start.4 = (bf16[24,2048]{1,0:T(8,128)(2,1)S(1)}, bf16[24,2048]{1,0:T(8,128)(2,1)S(1)}, u32[]{:S(2)}, u32[]{:S(2)}) collective-permute-start(bf16[24,2048]{1,0:T(8,128)(2,1)S(1)} %get-tuple-element.23), channel_id=1, source_target_pairs={{0,20},{4,24},{8,28},{12,0},{16,4},{20,8},{24,12},{28,16},{1,21},{... | collective-permute-start | bytes 294920 | tf_op jit(solution)/shard_map/ppermute | solution.py:12
  15.6 7.1 %collective-permute-start.5 = (bf16[24,2048]{1,0:T(8,128)(2,1)S(1)}, bf16[24,2048]{1,0:T(8,128)(2,1)S(1)}, u32[]{:S(2)}, u32[]{:S(2)}) collective-permute-start(bf16[24,2048]{1,0:T(8,128)(2,1)S(1)} %get-tuple-element.22), channel_id=1, source_target_pairs={{0,24},{4,28},{8,0},{12,4},{16,8},{20,12},{24,16},{28,20},{1,25},{... | collective-permute-start | bytes 294920 | tf_op jit(solution)/shard_map/ppermute | solution.py:12
  17.0 5.9 %collective-permute-start.6 = (bf16[24,2048]{1,0:T(8,128)(2,1)S(1)}, bf16[24,2048]{1,0:T(8,128)(2,1)S(1)}, u32[]{:S(2)}, u32[]{:S(2)}) collective-permute-start(bf16[24,2048]{1,0:T(8,128)(2,1)S(1)} %get-tuple-element.21), channel_id=1, source_target_pairs={{0,28},{4,0},{8,4},{12,8},{16,12},{20,16},{24,20},{28,24},{1,29},{... | collective-permute-start | bytes 294920 | tf_op jit(solution)/shard_map/ppermute | solution.py:12
  22.9 2.4 %collective-permute-start.7 = (bf16[192,2048]{1,0:T(8,128)(2,1)S(1)}, bf16[192,2048]{1,0:T(8,128)(2,1)S(1)}, u32[]{:S(2)}, u32[]{:S(2)}) collective-permute-start(bf16[192,2048]{1,0:T(8,128)(2,1)S(1)} %constant_dynamic-update-slice_fusion), channel_id=1, source_target_pairs={{0,1},{1,0},{2,3},{3,2},{4,5},{5,4},{6,7},{7,6},{8,9},{9,8},{10,11... | collective-permute-start | bytes 2359304 | tf_op jit(solution)/shard_map/ppermute | solution.py:12
  34.4 2.4 %collective-permute-start.8 = (bf16[192,2048]{1,0:T(8,128)(2,1)S(1)}, bf16[192,2048]{1,0:T(8,128)(2,1)S(1)}, u32[]{:S(2)}, u32[]{:S(2)}) collective-permute-start(bf16[192,2048]{1,0:T(8,128)(2,1)S(1)} %broadcast_select_fusion), channel_id=1, source_target_pairs={{0,1},{1,0},{2,3},{3,2},{4,5},{5,4},{6,7},{7,6},{8,9},{9,8},{10,11... | collective-permute-start | bytes 2359304 | tf_op jit(solution)/shard_map/ppermute | solution.py:12
  37.2 8.3 %copy-start.1 = (f32[32,4]{0,1:T(4,128)S(1)}, f32[32,4]{0,1:T(4,128)}, u32[]{:S(2)}) copy-start(f32[32,4]{0,1:T(4,128)} %param.10) | copy-start | bytes 1540
  37.2 12.9 %collective-permute-start.9 = (bf16[24,2048]{1,0:T(8,128)(2,1)S(1)}, bf16[24,2048]{1,0:T(8,128)(2,1)S(1)}, u32[]{:S(2)}, u32[]{:S(2)}) collective-permute-start(bf16[24,2048]{1,0:T(8,128)(2,1)S(1)} %get-tuple-element.19), channel_id=1, source_target_pairs={{0,28},{4,0},{8,4},{12,8},{16,12},{20,16},{24,20},{28,24},{1,29},{... | collective-permute-start | bytes 294920 | tf_op jit(solution)/shard_map/ppermute | solution.py:12
  45.6 6.6 %collective-permute-start.10 = (bf16[24,2048]{1,0:T(8,128)(2,1)S(1)}, bf16[24,2048]{1,0:T(8,128)(2,1)S(1)}, u32[]{:S(2)}, u32[]{:S(2)}) collective-permute-start(bf16[24,2048]{1,0:T(8,128)(2,1)S(1)} %get-tuple-element.18), channel_id=1, source_target_pairs={{0,24},{4,28},{8,0},{12,4},{16,8},{20,12},{24,16},{28,20},{1,25},{... | collective-permute-start | bytes 294920 | tf_op jit(solution)/shard_map/ppermute | solution.py:12
  47.2 6.1 %collective-permute-start.11 = (bf16[24,2048]{1,0:T(8,128)(2,1)S(1)}, bf16[24,2048]{1,0:T(8,128)(2,1)S(1)}, u32[]{:S(2)}, u32[]{:S(2)}) collective-permute-start(bf16[24,2048]{1,0:T(8,128)(2,1)S(1)} %get-tuple-element.17), channel_id=1, source_target_pairs={{0,20},{4,24},{8,28},{12,0},{16,4},{20,8},{24,12},{28,16},{1,21},{... | collective-permute-start | bytes 294920 | tf_op jit(solution)/shard_map/ppermute | solution.py:12
  47.2 16.5 %collective-permute-start.12 = (bf16[24,2048]{1,0:T(8,128)(2,1)S(1)}, bf16[24,2048]{1,0:T(8,128)(2,1)S(1)}, u32[]{:S(2)}, u32[]{:S(2)}) collective-permute-start(bf16[24,2048]{1,0:T(8,128)(2,1)S(1)} %get-tuple-element.16), channel_id=1, source_target_pairs={{0,16},{4,20},{8,24},{12,28},{16,0},{20,4},{24,8},{28,12},{1,17},{... | collective-permute-start | bytes 294920 | tf_op jit(solution)/shard_map/ppermute | solution.py:12
  49.1 16.0 %collective-permute-start.13 = (bf16[24,2048]{1,0:T(8,128)(2,1)S(1)}, bf16[24,2048]{1,0:T(8,128)(2,1)S(1)}, u32[]{:S(2)}, u32[]{:S(2)}) collective-permute-start(bf16[24,2048]{1,0:T(8,128)(2,1)S(1)} %get-tuple-element.15), channel_id=1, source_target_pairs={{0,12},{4,16},{8,20},{12,24},{16,28},{20,0},{24,4},{28,8},{1,13},{... | collective-permute-start | bytes 294920 | tf_op jit(solution)/shard_map/ppermute | solution.py:12
  50.1 15.0 %collective-permute-start.14 = (bf16[24,2048]{1,0:T(8,128)(2,1)S(1)}, bf16[24,2048]{1,0:T(8,128)(2,1)S(1)}, u32[]{:S(2)}, u32[]{:S(2)}) collective-permute-start(bf16[24,2048]{1,0:T(8,128)(2,1)S(1)} %get-tuple-element.14), channel_id=1, source_target_pairs={{0,8},{4,12},{8,16},{12,20},{16,24},{20,28},{24,0},{28,4},{1,9},{5... | collective-permute-start | bytes 294920 | tf_op jit(solution)/shard_map/ppermute | solution.py:12
  52.2 20.0 %copy-start = (f32[1024]{0:T(1024)S(1)}, f32[1024]{0:T(1024)}, u32[]{:S(2)}) copy-start(f32[1024]{0:T(1024)} %param.15) | copy-start | bytes 12292
  52.2 13.0 %collective-permute-start.15 = (bf16[24,2048]{1,0:T(8,128)(2,1)S(1)}, bf16[24,2048]{1,0:T(8,128)(2,1)S(1)}, u32[]{:S(2)}, u32[]{:S(2)}) collective-permute-start(bf16[24,2048]{1,0:T(8,128)(2,1)S(1)} %get-tuple-element.13), channel_id=1, source_target_pairs={{0,4},{4,8},{8,12},{12,16},{16,20},{20,24},{24,28},{28,0},{1,5},{5... | collective-permute-start | bytes 294920 | tf_op jit(solution)/shard_map/ppermute | solution.py:12
  65.7 5.0 %collective-permute-start.16 = (bf16[32,2048]{1,0:T(8,128)(2,1)S(1)}, bf16[32,2048]{1,0:T(8,128)(2,1)S(1)}, u32[]{:S(2)}, u32[]{:S(2)}) collective-permute-start(bf16[32,2048]{1,0:T(8,128)(2,1)S(1)} %get-tuple-element.29), channel_id=1, source_target_pairs={{0,2},{1,3},{2,0},{3,1},{4,6},{5,7},{6,4},{7,5},{8,10},{9,11},{10,... | collective-permute-start | bytes 393224 | tf_op jit(solution)/shard_map/ppermute | solution.py:12
  70.9 1.3 %collective-permute-start.17 = (f32[32,128]{0,1:T(8,128)S(1)}, f32[32,128]{0,1:T(8,128)S(1)}, u32[]{:S(2)}, u32[]{:S(2)}) collective-permute-start(f32[32,128]{0,1:T(8,128)S(1)} %broadcast_in_dim.16), channel_id=1, source_target_pairs={{0,1},{1,0},{2,3},{3,2},{4,5},{5,4},{6,7},{7,6},{8,9},{9,8},{10,11... | collective-permute-start | bytes 49160 | tf_op jit(solution)/shard_map/ppermute | solution.py:12

commit v2 on v1

v2 whole, which is shorter than its diff:
```python
import jax
import jax.numpy as jnp
from jax import lax
from jax.experimental import pallas as pl
from jax.experimental.pallas import tpu as pltpu
from jax.sharding import PartitionSpec as P

epsilon = 1e-06
direct_limit = 16


def send(value, axis, move):
    size = lax.axis_size(axis)
    return lax.ppermute(value, axis, [(i, move(i, size)) for i in range(size)])


def start_all(pairs, sems):
    copies = [pltpu.make_async_copy(src, dst, sems.at[i]) for i, (src, dst) in enumerate(pairs)]
    for copy in copies:
        copy.start()
    return copies


def select_body(core_ref, picked, gain, tokens_hbm, outgoing, token_buf, sems):
    half = token_buf.shape[2]
    copies = start_all(
        [(tokens_hbm.at[:, pl.ds(j * half, half)], token_buf.at[j]) for j in range(2)], sems
    )
    total = 0.0
    for j in range(2):
        copies[j].wait()
        floats = token_buf[j].astype(jnp.float32)
        total = total + jnp.sum(floats * floats, axis=1, keepdims=True)
    scale = lax.rsqrt(total / (2 * half) + epsilon)
    core = core_ref[0]
    own_gain = gain[pl.ds(core, 1), :]
    normed = (token_buf[core].astype(jnp.float32) * scale * own_gain).astype(jnp.bfloat16)
    outgoing[...] = lax.dot_general(
        picked[...], normed, (((0,), (0,)), ((), ())), preferred_element_type=jnp.float32
    ).astype(jnp.bfloat16)


def half_products(part, rows_hbm, gate_hbm, up_hbm, rows_buf, gate_buf, up_buf, sems, extra):
    half = rows_buf.shape[1]
    steps, chunk = gate_buf.shape[0], gate_buf.shape[1]
    pairs = [(rows_hbm, rows_buf)]
    for j in range(steps):
        rows = pl.ds(pl.multiple_of(part * half + j * chunk, chunk), chunk)
        pairs.append((gate_hbm.at[0, rows, :], gate_buf.at[j]))
        pairs.append((up_hbm.at[0, rows, :], up_buf.at[j]))
    copies = start_all(pairs + extra, sems)
    copies[0].wait()
    gate_act = up_act = 0.0
    for j in range(steps):
        rows = rows_buf[:, j * chunk : (j + 1) * chunk]
        copies[2 * j + 1].wait()
        gate_act = gate_act + jnp.dot(rows, gate_buf[j], preferred_element_type=jnp.float32)
        copies[2 * j + 2].wait()
        up_act = up_act + jnp.dot(rows, up_buf[j], preferred_element_type=jnp.float32)
    return gate_act, up_act, copies[2 * steps + 1 :]


def first_body(core_ref, rows_hbm, gate_hbm, up_hbm, gate_out, up_out, rows_buf, gate_buf, up_buf, sems):
    gate_out[...], up_out[...], _ = half_products(
        core_ref[0], rows_hbm, gate_hbm, up_hbm, rows_buf, gate_buf, up_buf, sems, []
    )


def down_pairs(part, down_hbm, down_buf):
    chips, piece = down_buf.shape[0], down_buf.shape[2]
    pairs = []
    for p in range(chips):
        start = pl.multiple_of((2 * p + part) * piece, piece)
        pairs.append((down_hbm.at[0, :, pl.ds(start, piece)], down_buf.at[p]))
    return pairs


def down_products(hidden, copies, down_buf, target):
    chips, piece = down_buf.shape[0], down_buf.shape[2]
    for p in range(chips):
        copies[p].wait()
        value = jnp.dot(hidden, down_buf[p], preferred_element_type=jnp.float32)
        target[:, p * piece : (p + 1) * piece] = value.astype(jnp.bfloat16)


def second_body(
    core_ref, gate_first, up_first, rows_hbm, gate_hbm, up_hbm, down_hbm, hidden_out, given,
    rows_buf, gate_buf, up_buf, down_buf, sems,
):
    other = 1 - core_ref[0]
    gate_act, up_act, copies = half_products(
        other, rows_hbm, gate_hbm, up_hbm, rows_buf, gate_buf, up_buf, sems,
        down_pairs(other, down_hbm, down_buf),
    )
    gate_act = gate_act + gate_first[...]
    up_act = up_act + up_first[...]
    hidden = (gate_act / (1.0 + jnp.exp(-gate_act)) * up_act).astype(jnp.bfloat16)
    hidden_out[...] = hidden
    down_products(hidden, copies, down_buf, given)


def third_body(core_ref, hidden, down_hbm, kept, down_buf, sems):
    copies = start_all(down_pairs(core_ref[0], down_hbm, down_buf), sems)
    down_products(hidden[...], copies, down_buf, kept)


smem = pl.BlockSpec(memory_space=pltpu.SMEM)
vmem = pl.BlockSpec(memory_space=pltpu.VMEM)
hbm = pl.BlockSpec(memory_space=pltpu.MemorySpace.HBM)


def in_hbm(value):
    return pltpu.with_memory_space_constraint(value, pltpu.MemorySpace.HBM)


def on_core(body, name, shapes, specs, scratch, copies):
    return pl.pallas_call(
        body,
        out_shape=tuple(jax.ShapeDtypeStruct(*shape) for shape in shapes),
        in_specs=[smem] + specs,
        out_specs=tuple(vmem for _ in shapes),
        scratch_shapes=[pltpu.VMEM(shape, jnp.bfloat16) for shape in scratch]
        + [pltpu.SemaphoreType.DMA((copies,))],
        compiler_params=pltpu.CompilerParams(vmem_limit_bytes=32 * 1024 * 1024),
        name=name,
    )


def run_expert(core, mine, gate_weight, up_weight, down_weight, piece):
    slots, half = mine.shape
    units = gate_weight.shape[2]
    chips = down_weight.shape[2] // (2 * piece)
    gate_weight, up_weight, down_weight = map(in_hbm, (gate_weight, up_weight, down_weight))
    steps = 2
    chunk = half // steps
    halves = [(slots, half), (steps, chunk, units), (steps, chunk, units)]
    downs = (chips, units, piece)
    acts = ((slots, units), jnp.float32)
    wide = ((slots, half), jnp.bfloat16)
    where = core.reshape(1).astype(jnp.int32)
    other = send(mine, "tp", lambda i, n: i ^ 1)
    gate_first, up_first = on_core(
        first_body, "first", (acts, acts), [hbm] * 3, halves, 2 * steps + 1
    )(where, mine, gate_weight, up_weight)
    hidden, given = on_core(
        second_body, "second", (((slots, units), jnp.bfloat16), wide), [vmem] * 2 + [hbm] * 4,
        halves + [downs], 2 * steps + 1 + chips,
    )(where, gate_first, up_first, other, gate_weight, up_weight, down_weight)
    gained = send(given, "tp", lambda i, n: i ^ 1)
    (kept,) = on_core(third_body, "third", (wide,), [vmem, hbm], [downs], chips)(
        where, hidden, down_weight
    )
    return kept, gained


def on_device(
    tokens, routes, mix_weights, pre_gain, gate_weight, up_weight, down_weight, post_gain
):
    tok_rows, width = tokens.shape
    top_count = routes.shape[1]
    experts = lax.axis_size("ep")
    shards = lax.axis_size("tp")
    chips = shards // 2
    piece = width // shards
    half = width // 2
    paired = False
    order = list(range(experts - 1, 0, -1))
    direct = experts <= direct_limit
    capacity = min(tok_rows, max(2, (3 * tok_rows * top_count + 2 * experts - 1) // (2 * experts)))
    slots = experts * capacity
    core = lax.axis_index("tp") % 2
    chip = lax.axis_index("tp") // 2

    def exchange(rows, back):
        if not direct:
            blocks = rows.reshape(experts, capacity, rows.shape[1])
            blocks = lax.all_to_all(blocks, "ep", split_axis=0, concat_axis=0, tiled=True)
            return blocks.reshape(rows.shape)
        sign = -1 if back else 1
        parts = {0: rows[:capacity]}
        for k in order:
            block = rows[k * capacity : (k + 1) * capacity]
            if paired:
                parts[k] = send(block, "ep", lambda i, n, k=k: i ^ k)
            else:
                parts[k] = send(block, "ep", lambda i, n, k=k: (i + sign * k) % n)
        return jnp.concatenate([parts[k] for k in range(experts)], axis=0)

    chosen = routes.reshape(-1)
    if direct:
        here = lax.axis_index("ep")
        chosen = chosen ^ here if paired else (chosen - here) % experts
    onehot = (chosen[:, None] == jnp.arange(experts, dtype=jnp.int32)[None, :]).astype(jnp.float32)
    count = tok_rows * top_count
    earlier = (
        jnp.arange(count, dtype=jnp.int32)[:, None] > jnp.arange(count, dtype=jnp.int32)[None, :]
    ).astype(jnp.float32)
    before = jnp.dot(earlier, onehot, preferred_element_type=jnp.float32)
    slot_rank = jnp.sum(before * onehot, axis=1).astype(jnp.int32)
    target = (chosen * capacity + slot_rank).reshape(tok_rows, top_count)
    by_choice = target[:, :, None] == jnp.arange(slots, dtype=jnp.int32)[None, None, :]
    picked = jnp.any(by_choice, axis=1).astype(jnp.bfloat16)
    mixing = jnp.sum(jnp.where(by_choice, mix_weights[:, :, None], 0.0), axis=1)

    (outgoing,) = on_core(
        select_body, "select", (((slots, half), jnp.bfloat16),), [vmem, vmem, hbm],
        [(2, tok_rows, half)], 2,
    )(core.reshape(1).astype(jnp.int32), picked, pre_gain.reshape(2, half), in_hbm(tokens))
    mine = exchange(outgoing, False)
    kept, gained = run_expert(core, mine, gate_weight, up_weight, down_weight, piece)
    chip_sum = (kept.astype(jnp.float32) + gained.astype(jnp.float32)).astype(jnp.bfloat16)
    returned = exchange(chip_sum, True)
    mixed_part = jnp.dot(mixing, returned.astype(jnp.float32), precision=lax.Precision.HIGHEST)
    mixed_sent = mixed_part.astype(jnp.bfloat16)
    mixed = mixed_part
    for k in range(1, chips):
        mixed = mixed + send(mixed_sent, "tp", lambda i, n, k=k: (i + 2 * k) % n).astype(jnp.float32)
    squares = jnp.sum(mixed * mixed, axis=1, keepdims=True)
    squares = jnp.broadcast_to(squares, (tok_rows, 128))
    total = squares + send(squares, "tp", lambda i, n: i ^ 1)
    scale_out = lax.rsqrt(total[:, :1] / width + epsilon)
    result = lax.dynamic_slice_in_dim(mixed, chip * piece, piece, 1)
    return (result * scale_out * post_gain).astype(jnp.bfloat16)


def solution(mesh):
    in_specs = (
        P("ep", None),
        P("ep", None),
        P("ep", None),
        P(),
        P("ep", None, "tp"),
        P("ep", None, "tp"),
        P("ep", "tp", None),
        P("tp"),
    )
    out_specs = P("ep", "tp")
    return jax.shard_map(
        on_device, mesh=mesh, in_specs=in_specs, out_specs=out_specs, check_vma=False
    )
```

time: 73.2 us -> 68.2 us (0.932)
  Pallas kernels: 0 us -> 10.6 us
  matrix products: 10.5 us -> 0.62 us
  waiting for transfers between devices: 25.8 us -> 22 us
  other arithmetic: 2.98 us -> 1.38 us
    pallas_call x0 -> x4, Pallas kernels: none -> 10.6 us  [the longest x1 3.93 us: run_expert(): on_core(second_body, 'second', (((slots, units), jnp.bfloat16), wide), [v...]
    dot_general x3 -> x0, matrix products: 9.92 us -> none  [the longest x1 5.42 us: on_device(): jnp.dot(hidden, down_weight[0], preferred_element_type=jnp.float32)]
    ppermute x18, waiting for transfers between devices: 25.8 us -> 22 us  [send(): return lax.ppermute(value, axis, [(i, move(i, size)) for i in range(size)])]
    reduce_sum x1 -> x0, other arithmetic: 1.11 us -> none  [on_device(): jnp.mean(floats * floats, axis=-1, keepdims=True) + epsilon]
    reshape x0 -> x1, local copies, waits for them, and re-layouts: none -> 0.73 us  [on_device(): pre_gain.reshape(2, half)]
  transfers between devices with their start and end apart: 18 -> 18, of which waited for: 10 -> 8; matrix products, arithmetic and copies ran while one was open for 0% -> 0% of each run, Pallas kernels for 0% -> 8%
where the time goes in v2:
time: 68.2 us; the launch traced here: 67.9 us
  starting transfers between devices  31 us (45%)
  waiting for transfers between devices  22 us (32%)
  Pallas kernels  10.6 us (16%)
  local copies, waits for them, and re-layouts  2.04 us (3%)
  other arithmetic  1.38 us (2%)
    ppermute x18, starting transfers between devices, send(): return lax.ppermute(value, axis, [(i, move(i, size)) for i in range(size)])  31 us
    ppermute x18, waiting for transfers between devices, send(): return lax.ppermute(value, axis, [(i, move(i, size)) for i in range(size)])  22 us
    pallas_call x1, Pallas kernels, run_expert(): on_core(second_body, 'second', (((slots, units), jnp.bfloat16), wide), [v...  3.93 us
    pallas_call x1, Pallas kernels, run_expert(): on_core(first_body, 'first', (acts, acts), [hbm] * 3, halves, 2 * steps + 1)  3.14 us
    pallas_call x1, Pallas kernels, run_expert(): on_core(third_body, 'third', (wide,), [vmem, hbm], [downs], chips)  2.02 us
    pallas_call x1, Pallas kernels, on_device(): on_core(select_body, 'select', (((slots, half), jnp.bfloat16),), [vmem, v...  1.49 us
  transfers between devices with their start and end apart: 18, of which 8 were waited for; matrix products, arithmetic and copies ran while one was open for 0% of the time, Pallas kernels for 8%

profile of v2, /device:TPU:0, one launch (start us, length us, event | category | flops | bytes accessed | tf_op | source)
XLA Modules:
  0.0 67.9 jit_solution(13004915723561388353)
XLA Ops:
  0.0 0.8 %copy.13 = s32[32,4]{1,0:T(8,128)S(1)} copy(s32[32,4]{0,1:T(4,128)} %param.9) | data formatting | bytes 1024 | tf_op args[1]
  2.1 1.5 %select.20 = bf16[192,2048]{1,0:T(8,128)(2,1)S(1)} custom-call(s32[1]{0:T(128)} %bitcast.core_ref, bf16[32,192]{1,0:T(8,128)(2,1)S(1)} %convert_element_type.34.picked, f32[2,2048]{1,0:T(2,128)S(1)} %reshape.50.gain, bf16[32,4096]{1,0:T(8,128)(2,1)} %tokens_hbm.1), custom_call_target="tpu_custom_call" | custom-call | tf_op jit(solution)/shard_map/select/pallas_call | solution.py:205
  3.7 3.0 %collective-permute-start = (bf16[24,2048]{1,0:T(8,128)(2,1)S(1)}, bf16[24,2048]{1,0:T(8,128)(2,1)S(1)}, u32[]{:S(2)}, u32[]{:S(2)}) collective-permute-start(bf16[24,2048]{1,0:T(8,128)(2,1)S(1)} %get-tuple-element.29), channel_id=1, source_target_pairs={{0,4},{4,8},{8,12},{12,16},{16,20},{20,24},{24,28},{28,0},{1,5},{5... | collective-permute-start | bytes 294920 | tf_op jit(solution)/shard_map/ppermute | solution.py:14
  6.7 1.6 %collective-permute-start.1 = (bf16[24,2048]{1,0:T(8,128)(2,1)S(1)}, bf16[24,2048]{1,0:T(8,128)(2,1)S(1)}, u32[]{:S(2)}, u32[]{:S(2)}) collective-permute-start(bf16[24,2048]{1,0:T(8,128)(2,1)S(1)} %get-tuple-element.28), channel_id=1, source_target_pairs={{0,8},{4,12},{8,16},{12,20},{16,24},{20,28},{24,0},{28,4},{1,9},{5... | collective-permute-start | bytes 294920 | tf_op jit(solution)/shard_map/ppermute | solution.py:14
  8.3 2.6 %collective-permute-start.2 = (bf16[24,2048]{1,0:T(8,128)(2,1)S(1)}, bf16[24,2048]{1,0:T(8,128)(2,1)S(1)}, u32[]{:S(2)}, u32[]{:S(2)}) collective-permute-start(bf16[24,2048]{1,0:T(8,128)(2,1)S(1)} %get-tuple-element.27), channel_id=1, source_target_pairs={{0,12},{4,16},{8,20},{12,24},{16,28},{20,0},{24,4},{28,8},{1,13},{... | collective-permute-start | bytes 294920 | tf_op jit(solution)/shard_map/ppermute | solution.py:14
  10.9 1.2 %collective-permute-start.3 = (bf16[24,2048]{1,0:T(8,128)(2,1)S(1)}, bf16[24,2048]{1,0:T(8,128)(2,1)S(1)}, u32[]{:S(2)}, u32[]{:S(2)}) collective-permute-start(bf16[24,2048]{1,0:T(8,128)(2,1)S(1)} %get-tuple-element.26), channel_id=1, source_target_pairs={{0,16},{4,20},{8,24},{12,28},{16,0},{20,4},{24,8},{28,12},{1,17},{... | collective-permute-start | bytes 294920 | tf_op jit(solution)/shard_map/ppermute | solution.py:14
  12.1 2.6 %collective-permute-start.4 = (bf16[24,2048]{1,0:T(8,128)(2,1)S(1)}, bf16[24,2048]{1,0:T(8,128)(2,1)S(1)}, u32[]{:S(2)}, u32[]{:S(2)}) collective-permute-start(bf16[24,2048]{1,0:T(8,128)(2,1)S(1)} %get-tuple-element.25), channel_id=1, source_target_pairs={{0,20},{4,24},{8,28},{12,0},{16,4},{20,8},{24,12},{28,16},{1,21},{... | collective-permute-start | bytes 294920 | tf_op jit(solution)/shard_map/ppermute | solution.py:14
  14.7 1.3 %collective-permute-start.5 = (bf16[24,2048]{1,0:T(8,128)(2,1)S(1)}, bf16[24,2048]{1,0:T(8,128)(2,1)S(1)}, u32[]{:S(2)}, u32[]{:S(2)}) collective-permute-start(bf16[24,2048]{1,0:T(8,128)(2,1)S(1)} %get-tuple-element.24), channel_id=1, source_target_pairs={{0,24},{4,28},{8,0},{12,4},{16,8},{20,12},{24,16},{28,20},{1,25},{... | collective-permute-start | bytes 294920 | tf_op jit(solution)/shard_map/ppermute | solution.py:14
  16.1 1.5 %collective-permute-start.6 = (bf16[24,2048]{1,0:T(8,128)(2,1)S(1)}, bf16[24,2048]{1,0:T(8,128)(2,1)S(1)}, u32[]{:S(2)}, u32[]{:S(2)}) collective-permute-start(bf16[24,2048]{1,0:T(8,128)(2,1)S(1)} %get-tuple-element.23), channel_id=1, source_target_pairs={{0,28},{4,0},{8,4},{12,8},{16,12},{20,16},{24,20},{28,24},{1,29},{... | collective-permute-start | bytes 294920 | tf_op jit(solution)/shard_map/ppermute | solution.py:14
  17.6 3.6 %collective-permute-done.2 = bf16[24,2048]{1,0:T(8,128)(2,1)S(1)} collective-permute-done((bf16[24,2048]{1,0:T(8,128)(2,1)S(1)}, bf16[24,2048]{1,0:T(8,128)(2,1)S(1)}, u32[]{:S(2)}, u32[]{:S(2)}) %collective-permute-start.2) | collective-permute-done | bytes 98336 | tf_op jit(solution)/shard_map/ppermute | solution.py:14
  22.1 3.1 %first.1 = (f32[192,512]{1,0:T(8,128)S(1)}, f32[192,512]{1,0:T(8,128)S(1)}) custom-call(s32[1]{0:T(128)} %bitcast.core_ref, bf16[192,2048]{1,0:T(8,128)(2,1)S(1)} %constant_dynamic-update-slice_fusion.rows_hbm, bf16[1,4096,512]{2,1,0:T(8,128)(2,1)} %gate_hbm.3, bf16[1,4096,512]{2,1,0:T(8,128)(2,1)} %up_hbm.3), custom_call_target="tpu_custom_call" | custom-call | tf_op jit(solution)/shard_map/first/pallas_call | solution.py:142
  25.3 3.9 %second.1 = (bf16[192,512]{1,0:T(8,128)(2,1)S(1)}, bf16[192,2048]{1,0:T(8,128)(2,1)S(1)}) custom-call(s32[1]{0:T(128)} %bitcast.core_ref, f32[192,512]{1,0:T(8,128)S(1)} %get-tuple-element.9.gate_first, f32[192,512]{1,0:T(8,128)S(1)} %get-tuple-element.10.up_first, bf16[192,2048]{1,0:T(8,128)(2,1)S(1)} %collective-permute-done.7.rows_hbm, ...), custom_call_target="tpu_custom_call" | custom-call | tf_op jit(solution)/shard_map/second/pallas_call | solution.py:145
  29.8 2.0 %third.1 = bf16[192,2048]{1,0:T(8,128)(2,1)S(1)} custom-call(s32[1]{0:T(128)} %bitcast.core_ref, bf16[192,512]{1,0:T(8,128)(2,1)S(1)} %get-tuple-element.11.hidden, bf16[1,512,4096]{2,1,0:T(8,128)(2,1)} %down_hbm.3), custom_call_target="tpu_custom_call" | custom-call | tf_op jit(solution)/shard_map/third/pallas_call | solution.py:150
  32.1 8.2 %collective-permute-start.9 = (bf16[24,2048]{1,0:T(8,128)(2,1)S(1)}, bf16[24,2048]{1,0:T(8,128)(2,1)S(1)}, u32[]{:S(2)}, u32[]{:S(2)}) collective-permute-start(bf16[24,2048]{1,0:T(8,128)(2,1)S(1)} %get-tuple-element.21), channel_id=1, source_target_pairs={{0,28},{4,0},{8,4},{12,8},{16,12},{20,16},{24,20},{28,24},{1,29},{... | collective-permute-start | bytes 294920 | tf_op jit(solution)/shard_map/ppermute | solution.py:14
  40.5 1.6 %collective-permute-start.10 = (bf16[24,2048]{1,0:T(8,128)(2,1)S(1)}, bf16[24,2048]{1,0:T(8,128)(2,1)S(1)}, u32[]{:S(2)}, u32[]{:S(2)}) collective-permute-start(bf16[24,2048]{1,0:T(8,128)(2,1)S(1)} %get-tuple-element.20), channel_id=1, source_target_pairs={{0,24},{4,28},{8,0},{12,4},{16,8},{20,12},{24,16},{28,20},{1,25},{... | collective-permute-start | bytes 294920 | tf_op jit(solution)/shard_map/ppermute | solution.py:14
  42.1 1.4 %collective-permute-start.12 = (bf16[24,2048]{1,0:T(8,128)(2,1)S(1)}, bf16[24,2048]{1,0:T(8,128)(2,1)S(1)}, u32[]{:S(2)}, u32[]{:S(2)}) collective-permute-start(bf16[24,2048]{1,0:T(8,128)(2,1)S(1)} %get-tuple-element.18), channel_id=1, source_target_pairs={{0,16},{4,20},{8,24},{12,28},{16,0},{20,4},{24,8},{28,12},{1,17},{... | collective-permute-start | bytes 294920 | tf_op jit(solution)/shard_map/ppermute | solution.py:14
  43.5 1.5 %collective-permute-start.13 = (bf16[24,2048]{1,0:T(8,128)(2,1)S(1)}, bf16[24,2048]{1,0:T(8,128)(2,1)S(1)}, u32[]{:S(2)}, u32[]{:S(2)}) collective-permute-start(bf16[24,2048]{1,0:T(8,128)(2,1)S(1)} %get-tuple-element.17), channel_id=1, source_target_pairs={{0,12},{4,16},{8,20},{12,24},{16,28},{20,0},{24,4},{28,8},{1,13},{... | collective-permute-start | bytes 294920 | tf_op jit(solution)/shard_map/ppermute | solution.py:14
  45.0 2.0 %collective-permute-start.14 = (bf16[24,2048]{1,0:T(8,128)(2,1)S(1)}, bf16[24,2048]{1,0:T(8,128)(2,1)S(1)}, u32[]{:S(2)}, u32[]{:S(2)}) collective-permute-start(bf16[24,2048]{1,0:T(8,128)(2,1)S(1)} %get-tuple-element.16), channel_id=1, source_target_pairs={{0,8},{4,12},{8,16},{12,20},{16,24},{20,28},{24,0},{28,4},{1,9},{5... | collective-permute-start | bytes 294920 | tf_op jit(solution)/shard_map/ppermute | solution.py:14
  47.2 0.9 %collective-permute-done.11 = bf16[24,2048]{1,0:T(8,128)(2,1)S(1)} collective-permute-done((bf16[24,2048]{1,0:T(8,128)(2,1)S(1)}, bf16[24,2048]{1,0:T(8,128)(2,1)S(1)}, u32[]{:S(2)}, u32[]{:S(2)}) %collective-permute-start.11) | collective-permute-done | bytes 98336 | tf_op jit(solution)/shard_map/ppermute | solution.py:14
  48.1 10.6 %collective-permute-done.12 = bf16[24,2048]{1,0:T(8,128)(2,1)S(1)} collective-permute-done((bf16[24,2048]{1,0:T(8,128)(2,1)S(1)}, bf16[24,2048]{1,0:T(8,128)(2,1)S(1)}, u32[]{:S(2)}, u32[]{:S(2)}) %collective-permute-start.12) | collective-permute-done | bytes 98336 | tf_op jit(solution)/shard_map/ppermute | solution.py:14
  58.7 1.4 %collective-permute-done.13 = bf16[24,2048]{1,0:T(8,128)(2,1)S(1)} collective-permute-done((bf16[24,2048]{1,0:T(8,128)(2,1)S(1)}, bf16[24,2048]{1,0:T(8,128)(2,1)S(1)}, u32[]{:S(2)}, u32[]{:S(2)}) %collective-permute-start.13) | collective-permute-done | bytes 98336 | tf_op jit(solution)/shard_map/ppermute | solution.py:14
  60.7 1.6 %collective-permute-start.16 = (bf16[32,2048]{1,0:T(8,128)(2,1)S(1)}, bf16[32,2048]{1,0:T(8,128)(2,1)S(1)}, u32[]{:S(2)}, u32[]{:S(2)}) collective-permute-start(bf16[32,2048]{1,0:T(8,128)(2,1)S(1)} %get-tuple-element.31), channel_id=1, source_target_pairs={{0,2},{1,3},{2,0},{3,1},{4,6},{5,7},{6,4},{7,5},{8,10},{9,11},{10,... | collective-permute-start | bytes 393224 | tf_op jit(solution)/shard_map/ppermute | solution.py:14
  62.3 3.4 %collective-permute-done.16 = bf16[32,2048]{1,0:T(8,128)(2,1)S(1)} collective-permute-done((bf16[32,2048]{1,0:T(8,128)(2,1)S(1)}, bf16[32,2048]{1,0:T(8,128)(2,1)S(1)}, u32[]{:S(2)}, u32[]{:S(2)}) %collective-permute-start.16) | collective-permute-done | bytes 131104 | tf_op jit(solution)/shard_map/ppermute | solution.py:14
  66.0 1.2 %collective-permute-done.17 = f32[32,128]{0,1:T(8,128)S(1)} collective-permute-done((f32[32,128]{0,1:T(8,128)S(1)}, f32[32,128]{0,1:T(8,128)S(1)}, u32[]{:S(2)}, u32[]{:S(2)}) %collective-permute-start.17) | collective-permute-done | bytes 16416 | tf_op jit(solution)/shard_map/ppermute | solution.py:14
  (55 shorter events, 4.8 us)
Async XLA Ops:
  3.7 11.0 %collective-permute-start = (bf16[24,2048]{1,0:T(8,128)(2,1)S(1)}, bf16[24,2048]{1,0:T(8,128)(2,1)S(1)}, u32[]{:S(2)}, u32[]{:S(2)}) collective-permute-start(bf16[24,2048]{1,0:T(8,128)(2,1)S(1)} %get-tuple-element.29), channel_id=1, source_target_pairs={{0,4},{4,8},{8,12},{12,16},{16,20},{20,24},{24,28},{28,0},{1,5},{5... | collective-permute-start | bytes 294920 | tf_op jit(solution)/shard_map/ppermute | solution.py:14
  6.7 9.3 %collective-permute-start.1 = (bf16[24,2048]{1,0:T(8,128)(2,1)S(1)}, bf16[24,2048]{1,0:T(8,128)(2,1)S(1)}, u32[]{:S(2)}, u32[]{:S(2)}) collective-permute-start(bf16[24,2048]{1,0:T(8,128)(2,1)S(1)} %get-tuple-element.28), channel_id=1, source_target_pairs={{0,8},{4,12},{8,16},{12,20},{16,24},{20,28},{24,0},{28,4},{1,9},{5... | collective-permute-start | bytes 294920 | tf_op jit(solution)/shard_map/ppermute | solution.py:14
  8.3 12.9 %collective-permute-start.2 = (bf16[24,2048]{1,0:T(8,128)(2,1)S(1)}, bf16[24,2048]{1,0:T(8,128)(2,1)S(1)}, u32[]{:S(2)}, u32[]{:S(2)}) collective-permute-start(bf16[24,2048]{1,0:T(8,128)(2,1)S(1)} %get-tuple-element.27), channel_id=1, source_target_pairs={{0,12},{4,16},{8,20},{12,24},{16,28},{20,0},{24,4},{28,8},{1,13},{... | collective-permute-start | bytes 294920 | tf_op jit(solution)/shard_map/ppermute | solution.py:14
  10.9 10.9 %collective-permute-start.3 = (bf16[24,2048]{1,0:T(8,128)(2,1)S(1)}, bf16[24,2048]{1,0:T(8,128)(2,1)S(1)}, u32[]{:S(2)}, u32[]{:S(2)}) collective-permute-start(bf16[24,2048]{1,0:T(8,128)(2,1)S(1)} %get-tuple-element.26), channel_id=1, source_target_pairs={{0,16},{4,20},{8,24},{12,28},{16,0},{20,4},{24,8},{28,12},{1,17},{... | collective-permute-start | bytes 294920 | tf_op jit(solution)/shard_map/ppermute | solution.py:14
  12.1 9.7 %collective-permute-start.4 = (bf16[24,2048]{1,0:T(8,128)(2,1)S(1)}, bf16[24,2048]{1,0:T(8,128)(2,1)S(1)}, u32[]{:S(2)}, u32[]{:S(2)}) collective-permute-start(bf16[24,2048]{1,0:T(8,128)(2,1)S(1)} %get-tuple-element.25), channel_id=1, source_target_pairs={{0,20},{4,24},{8,28},{12,0},{16,4},{20,8},{24,12},{28,16},{1,21},{... | collective-permute-start | bytes 294920 | tf_op jit(solution)/shard_map/ppermute | solution.py:14
  14.7 7.1 %collective-permute-start.5 = (bf16[24,2048]{1,0:T(8,128)(2,1)S(1)}, bf16[24,2048]{1,0:T(8,128)(2,1)S(1)}, u32[]{:S(2)}, u32[]{:S(2)}) collective-permute-start(bf16[24,2048]{1,0:T(8,128)(2,1)S(1)} %get-tuple-element.24), channel_id=1, source_target_pairs={{0,24},{4,28},{8,0},{12,4},{16,8},{20,12},{24,16},{28,20},{1,25},{... | collective-permute-start | bytes 294920 | tf_op jit(solution)/shard_map/ppermute | solution.py:14
  16.1 5.9 %collective-permute-start.6 = (bf16[24,2048]{1,0:T(8,128)(2,1)S(1)}, bf16[24,2048]{1,0:T(8,128)(2,1)S(1)}, u32[]{:S(2)}, u32[]{:S(2)}) collective-permute-start(bf16[24,2048]{1,0:T(8,128)(2,1)S(1)} %get-tuple-element.23), channel_id=1, source_target_pairs={{0,28},{4,0},{8,4},{12,8},{16,12},{20,16},{24,20},{28,24},{1,29},{... | collective-permute-start | bytes 294920 | tf_op jit(solution)/shard_map/ppermute | solution.py:14
  22.0 3.2 %collective-permute-start.7 = (bf16[192,2048]{1,0:T(8,128)(2,1)S(1)}, bf16[192,2048]{1,0:T(8,128)(2,1)S(1)}, u32[]{:S(2)}, u32[]{:S(2)}) collective-permute-start(bf16[192,2048]{1,0:T(8,128)(2,1)S(1)} %constant_dynamic-update-slice_fusion.rows_hbm), channel_id=1, source_target_pairs={{0,1},{1,0},{2,3},{3,2},{4,5},{5,4},{6,7},{7,6},{8,9},{9,8},{10,11... | collective-permute-start | bytes 2359304 | tf_op jit(solution)/shard_map/ppermute | solution.py:14
  29.2 2.6 %collective-permute-start.8 = (bf16[192,2048]{1,0:T(8,128)(2,1)S(1)}, bf16[192,2048]{1,0:T(8,128)(2,1)S(1)}, u32[]{:S(2)}, u32[]{:S(2)}) collective-permute-start(bf16[192,2048]{1,0:T(8,128)(2,1)S(1)} %get-tuple-element.12), channel_id=1, source_target_pairs={{0,1},{1,0},{2,3},{3,2},{4,5},{5,4},{6,7},{7,6},{8,9},{9,8},{10,11... | collective-permute-start | bytes 2359304 | tf_op jit(solution)/shard_map/ppermute | solution.py:14
  29.8 10.6 %copy-start.1 = (f32[32,4]{0,1:T(4,128)S(1)}, f32[32,4]{0,1:T(4,128)}, u32[]{:S(2)}) copy-start(f32[32,4]{0,1:T(4,128)} %param.10) | copy-start | bytes 1540
  31.8 35.4 %copy-start = (f32[1024]{0:T(1024)S(1)}, f32[1024]{0:T(1024)}, u32[]{:S(2)}) copy-start(f32[1024]{0:T(1024)} %param.15) | copy-start | bytes 12292
  32.1 12.9 %collective-permute-start.9 = (bf16[24,2048]{1,0:T(8,128)(2,1)S(1)}, bf16[24,2048]{1,0:T(8,128)(2,1)S(1)}, u32[]{:S(2)}, u32[]{:S(2)}) collective-permute-start(bf16[24,2048]{1,0:T(8,128)(2,1)S(1)} %get-tuple-element.21), channel_id=1, source_target_pairs={{0,28},{4,0},{8,4},{12,8},{16,12},{20,16},{24,20},{28,24},{1,29},{... | collective-permute-start | bytes 294920 | tf_op jit(solution)/shard_map/ppermute | solution.py:14
  40.5 6.6 %collective-permute-start.10 = (bf16[24,2048]{1,0:T(8,128)(2,1)S(1)}, bf16[24,2048]{1,0:T(8,128)(2,1)S(1)}, u32[]{:S(2)}, u32[]{:S(2)}) collective-permute-start(bf16[24,2048]{1,0:T(8,128)(2,1)S(1)} %get-tuple-element.20), channel_id=1, source_target_pairs={{0,24},{4,28},{8,0},{12,4},{16,8},{20,12},{24,16},{28,20},{1,25},{... | collective-permute-start | bytes 294920 | tf_op jit(solution)/shard_map/ppermute | solution.py:14
  42.1 6.0 %collective-permute-start.11 = (bf16[24,2048]{1,0:T(8,128)(2,1)S(1)}, bf16[24,2048]{1,0:T(8,128)(2,1)S(1)}, u32[]{:S(2)}, u32[]{:S(2)}) collective-permute-start(bf16[24,2048]{1,0:T(8,128)(2,1)S(1)} %get-tuple-element.19), channel_id=1, source_target_pairs={{0,20},{4,24},{8,28},{12,0},{16,4},{20,8},{24,12},{28,16},{1,21},{... | collective-permute-start | bytes 294920 | tf_op jit(solution)/shard_map/ppermute | solution.py:14
  42.1 16.6 %collective-permute-start.12 = (bf16[24,2048]{1,0:T(8,128)(2,1)S(1)}, bf16[24,2048]{1,0:T(8,128)(2,1)S(1)}, u32[]{:S(2)}, u32[]{:S(2)}) collective-permute-start(bf16[24,2048]{1,0:T(8,128)(2,1)S(1)} %get-tuple-element.18), channel_id=1, source_target_pairs={{0,16},{4,20},{8,24},{12,28},{16,0},{20,4},{24,8},{28,12},{1,17},{... | collective-permute-start | bytes 294920 | tf_op jit(solution)/shard_map/ppermute | solution.py:14
  43.5 16.7 %collective-permute-start.13 = (bf16[24,2048]{1,0:T(8,128)(2,1)S(1)}, bf16[24,2048]{1,0:T(8,128)(2,1)S(1)}, u32[]{:S(2)}, u32[]{:S(2)}) collective-permute-start(bf16[24,2048]{1,0:T(8,128)(2,1)S(1)} %get-tuple-element.17), channel_id=1, source_target_pairs={{0,12},{4,16},{8,20},{12,24},{16,28},{20,0},{24,4},{28,8},{1,13},{... | collective-permute-start | bytes 294920 | tf_op jit(solution)/shard_map/ppermute | solution.py:14
  45.0 15.1 %collective-permute-start.14 = (bf16[24,2048]{1,0:T(8,128)(2,1)S(1)}, bf16[24,2048]{1,0:T(8,128)(2,1)S(1)}, u32[]{:S(2)}, u32[]{:S(2)}) collective-permute-start(bf16[24,2048]{1,0:T(8,128)(2,1)S(1)} %get-tuple-element.16), channel_id=1, source_target_pairs={{0,8},{4,12},{8,16},{12,20},{16,24},{20,28},{24,0},{28,4},{1,9},{5... | collective-permute-start | bytes 294920 | tf_op jit(solution)/shard_map/ppermute | solution.py:14
  47.1 13.1 %collective-permute-start.15 = (bf16[24,2048]{1,0:T(8,128)(2,1)S(1)}, bf16[24,2048]{1,0:T(8,128)(2,1)S(1)}, u32[]{:S(2)}, u32[]{:S(2)}) collective-permute-start(bf16[24,2048]{1,0:T(8,128)(2,1)S(1)} %get-tuple-element.15), channel_id=1, source_target_pairs={{0,4},{4,8},{8,12},{12,16},{16,20},{20,24},{24,28},{28,0},{1,5},{5... | collective-permute-start | bytes 294920 | tf_op jit(solution)/shard_map/ppermute | solution.py:14
  60.7 5.0 %collective-permute-start.16 = (bf16[32,2048]{1,0:T(8,128)(2,1)S(1)}, bf16[32,2048]{1,0:T(8,128)(2,1)S(1)}, u32[]{:S(2)}, u32[]{:S(2)}) collective-permute-start(bf16[32,2048]{1,0:T(8,128)(2,1)S(1)} %get-tuple-element.31), channel_id=1, source_target_pairs={{0,2},{1,3},{2,0},{3,1},{4,6},{5,7},{6,4},{7,5},{8,10},{9,11},{10,... | collective-permute-start | bytes 393224 | tf_op jit(solution)/shard_map/ppermute | solution.py:14
  65.9 1.3 %collective-permute-start.17 = (f32[32,128]{0,1:T(8,128)S(1)}, f32[32,128]{0,1:T(8,128)S(1)}, u32[]{:S(2)}, u32[]{:S(2)}) collective-permute-start(f32[32,128]{0,1:T(8,128)S(1)} %broadcast_in_dim.16), channel_id=1, source_target_pairs={{0,1},{1,0},{2,3},{3,2},{4,5},{5,4},{6,7},{7,6},{8,9},{9,8},{10,11... | collective-permute-start | bytes 49160 | tf_op jit(solution)/shard_map/ppermute | solution.py:14
